TPU v7x, 32 devices: a whole 2x2x4 slice. The times are simulated.
32 devices in a mesh: sp: 8 (over z, x), tp: 4 (over y, core).
Axes of the slice: x: 2, y: 2, z: 4, core: 2. Of those that a mesh axis runs over, the one named last changes fastest.
Arguments:
- residual_signal: bfloat16 [1024, 2048], P('sp', 'tp'), may hold values from -90 to 90
- lifted_signal: bfloat16 [1024, 1024], P('sp', 'tp'), may hold values from -6 to 6
- discrete_timestep: float32 [64, 1024], P('tp', 'sp'), may hold values from 0.17 to 4.2
- additional_log_fading: float32 [64, 1024], P('tp', 'sp'), may hold values from -2.1 to 0
- paired_fading: float32 [2, 32, 64], replicated, may hold values from 1.953125e-05 to 0.0625
- unpaired_fading: float32 [2, 32, 32], replicated, may hold values from 1.953125e-05 to 0.0625
- paired_twist: float32 [2, 32, 64], replicated, may hold values from -3.140625 to 3.140625
- unpaired_twist: float32 [2, 32, 32], replicated, may hold values from -3.140625 to 3.140625
- paired_latent_linears: float32 [2, 2, 2, 32, 64, 16], replicated, may hold values from -1 to 1
- unpaired_latent_linears: float32 [2, 2, 2, 32, 32, 16], replicated, may hold values from -1 to 1
- skip_coefficient: float32 [1024], replicated, may hold values from -4 to 4
- closing_norm_multiplier: float32 [1024], replicated, may hold values from 0.1 to 1.9
- emitted_linear: bfloat16 [1024, 2048], replicated, may hold values from -0.1875 to 0.1875
- leading_norm_multiplier: float32 [2048], replicated, may hold values from 0.1 to 1.9
- raising_linear: bfloat16 [2048, 8192], P('sp', 'tp'), may hold values from -0.125 to 0.125
- lowering_linear: bfloat16 [8192, 2048], P('tp', 'sp'), may hold values from -0.0625 to 0.0625
Outputs:
- layer_out: bfloat16 [1024, 2048], P('sp', 'tp')
All inputs are finite; a program needn't handle non-finite values.
Results may differ from a plain program's by a relative error of at most 0.008.
Values may be sent and summed in bfloat16 or wider, within the bound.
A program may use at most 128 MiB of HBM per device.

v0:
```python
import functools

import jax
import jax.numpy as jnp
from jax import lax
from jax.experimental import pallas as pl
from jax.experimental.pallas import tpu as pltpu
from jax.sharding import PartitionSpec as P

CHAN = 16
NORM_W = 128
EPSILON = 1e-06
SUB = 8
F32, BF16 = jnp.float32, jnp.bfloat16


def sincos(a):
    k = jnp.floor(a * 0.6366197723675814 + 0.5)
    r = a - k * 1.5703125
    r = r - k * 4.8351287841796875e-4
    r = r - k * 3.138556210e-7
    z = r * r
    s = r + r * z * (-1.6666654611e-1 + z * (8.3321608736e-3 + z * -1.9515295891e-4))
    c = 1.0 - 0.5 * z + z * z * (
        4.166664568298827e-2 + z * (-1.388731625493765e-3 + z * 2.443315711809948e-5)
    )
    half = jnp.floor(k * 0.5)
    odd = (k - 2.0 * half) > 0.5
    half_odd = (half - 2.0 * jnp.floor(half * 0.5)) > 0.5
    cos_v = jnp.where(odd, -s, c)
    sin_v = jnp.where(odd, c, s)
    return jnp.where(half_odd, -cos_v, cos_v), jnp.where(half_odd, -sin_v, sin_v)


def one_minus_exp_neg(u):
    t = jnp.full_like(u, 1.0)
    for m in range(10, 1, -1):
        t = 1.0 - u * (1.0 / m) * t
    return u * t


def cmul(ar, ai, br, bi):
    return ar * br - ai * bi, ar * bi + ai * br


def mixer_body(cfg, x_ref, dt_ref, lf_ref, rates_ref, lin_ref, skip_ref, gain_ref,
               resid_ref, lead_ref, emit_hbm, mid_out, normed_out,
               pace, surge, pre, st, blk, ends, ends_all, cin, mg, rows_in, mrg, emit, resid_in,
               copy_sem, s_ends, r_ends, s_rows, r_rows, s_res, r_res):
    nsp, ntp, n, S, W, G, PL, PS, D = cfg
    L = n // SUB
    half = G // 2
    SL = half * PL
    sp = lax.axis_index("sp")
    tp = lax.axis_index("tp")
    q = n // ntp
    Dl = D // ntp
    MESH = pl.DeviceIdType.MESH

    emit_copy = pltpu.make_async_copy(emit_hbm, emit, copy_sem.at[0])
    emit_copy.start()
    barrier = pltpu.get_barrier_semaphore()
    for k in range(1, nsp):
        pl.semaphore_signal(barrier, inc=1, device_id=(lax.rem(sp + k, nsp), tp), device_id_type=MESH)
    for k in range(1, ntp):
        pl.semaphore_signal(barrier, inc=1, device_id=(sp, lax.rem(tp + k, ntp)), device_id_type=MESH)
    pl.semaphore_wait(barrier, nsp + ntp - 2)

    def res_copy(k):
        to = lax.rem(tp + k, ntp)
        return pltpu.make_async_remote_copy(
            src_ref=resid_ref.at[pl.ds(to * q, q), :], dst_ref=resid_in.at[k - 1],
            send_sem=s_res.at[k - 1], recv_sem=r_res.at[k - 1],
            device_id=(sp, to), device_id_type=MESH)

    for k in range(1, ntp):
        res_copy(k).start()

    lane = lax.broadcasted_iota(jnp.int32, (G, S), 1)
    group = jnp.where(lane < SL, 2 * (lane // PL), 2 * ((lane - SL) // PS) + 1)
    spread = (group == lax.broadcasted_iota(jnp.int32, (G, S), 0)).astype(F32)
    pace[...] = jnp.dot(dt_ref[...], spread, precision=lax.Precision.HIGHEST, preferred_element_type=F32)
    surge[...] = jnp.dot(lf_ref[...], spread, precision=lax.Precision.HIGHEST, preferred_element_type=F32)

    row = lax.broadcasted_iota(jnp.int32, (S, W), 0)
    row_group = jnp.where(row < SL, 2 * (row // PL), 2 * ((row - SL) // PS) + 1)
    mask = row_group == lax.broadcasted_iota(jnp.int32, (S, W), 1) // CHAN
    tile = (lax.broadcasted_iota(jnp.int32, (CHAN, W), 1) % CHAN
            == lax.broadcasted_iota(jnp.int32, (CHAN, W), 0)).astype(BF16)

    def block_map(index, sign=1.0):
        wide = jnp.dot(lin_ref[index].astype(BF16), tile, preferred_element_type=F32)
        return jnp.where(mask, sign * wide, 0.0).astype(BF16)

    xv = x_ref[...]
    for e in range(2):
        for c in range(2):
            st[:, pl.ds((2 * e + c) * S, S)] = lax.dot_general(
                xv, block_map(4 * e + c), (((1,), (1,)), ((), ())), preferred_element_type=F32)

    for e in range(2):
        rate = rates_ref[2 * e : 2 * e + 1, :]
        freq = rates_ref[2 * e + 1 : 2 * e + 2, :]

        def step(i, carry):
            pr, pi, sr, si = carry
            at = i if e == 0 else L - 1 - i
            rows = pl.ds(pl.multiple_of(at * SUB, SUB), SUB)
            d = pace[rows, :]
            rd = rate * d
            m = jnp.exp(surge[rows, :] - rd)
            cos_v, sin_v = sincos(freq * d)
            w = jnp.sqrt(one_minus_exp_neg(2.0 * rd))
            ar, ai = m * cos_v, m * sin_v
            pr, pi = cmul(ar, ai, pr, pi)
            sr, si = cmul(ar, ai, sr, si)
            sr = sr + w * st[rows, pl.ds(2 * e * S, S)]
            si = si + w * st[rows, pl.ds((2 * e + 1) * S, S)]
            pre[rows, pl.ds(2 * e * S, S)] = pr
            pre[rows, pl.ds((2 * e + 1) * S, S)] = pi
            st[rows, pl.ds(2 * e * S, S)] = sr
            st[rows, pl.ds((2 * e + 1) * S, S)] = si
            return pr, pi, sr, si

        zero = jnp.zeros((SUB, S), F32)
        total = lax.fori_loop(0, L, step, (zero + 1.0, zero, zero, zero))
        for c in range(4):
            blk[4 * e + c] = total[c]
        order = range(SUB) if e == 0 else range(SUB - 1, -1, -1)
        run = None
        for b in order:
            now = tuple(blk[4 * e + c, b : b + 1, :] for c in range(4))
            if run is None:
                run = now
            else:
                p = cmul(now[0], now[1], run[0], run[1])
                s = cmul(now[0], now[1], run[2], run[3])
                run = (p[0], p[1], s[0] + now[2], s[1] + now[3])
        for c in range(4):
            ends[4 * e + c : 4 * e + c + 1, :] = run[c]

    def ends_copy(k):
        return pltpu.make_async_remote_copy(
            src_ref=ends, dst_ref=ends_all.at[k - 1],
            send_sem=s_ends.at[k - 1], recv_sem=r_ends.at[k - 1],
            device_id=(lax.rem(sp + k, nsp), tp), device_id_type=MESH)

    for k in range(1, nsp):
        ends_copy(k).start()

    read = jnp.concatenate(
        [block_map(2), block_map(3, -1.0), block_map(6), block_map(7, -1.0)], axis=0)

    for k in range(1, nsp):
        ends_copy(k).wait_recv()
    blank = jnp.zeros((1, S), F32)

    def fold(j, carry, e):
        cr, ci = carry
        k = nsp - 1 - j if e == 0 else j + 1
        reached = k <= sp if e == 0 else nsp - k <= nsp - 1 - sp
        got = ends_all[k - 1]
        nr, ni = cmul(got[4 * e : 4 * e + 1], got[4 * e + 1 : 4 * e + 2], cr, ci)
        nr = nr + got[4 * e + 2 : 4 * e + 3]
        ni = ni + got[4 * e + 3 : 4 * e + 4]
        return jnp.where(reached, nr, cr), jnp.where(reached, ni, ci)

    for e in range(2):
        cr, ci = lax.fori_loop(0, nsp - 1, functools.partial(fold, e=e), (blank, blank))
        order = range(SUB) if e == 0 else range(SUB - 1, -1, -1)
        for b in order:
            cin[2 * e, b : b + 1, :] = cr
            cin[2 * e + 1, b : b + 1, :] = ci
            now = tuple(blk[4 * e + c, b : b + 1, :] for c in range(4))
            nr, ni = cmul(now[0], now[1], cr, ci)
            cr, ci = nr + now[2], ni + now[3]

        inr, ini = cin[2 * e], cin[2 * e + 1]

        def settle(i, _):
            rows = pl.ds(pl.multiple_of(i * SUB, SUB), SUB)
            re, im = pl.ds(2 * e * S, S), pl.ds((2 * e + 1) * S, S)
            ar, ai = cmul(pre[rows, re], pre[rows, im], inr, ini)
            st[rows, re] = st[rows, re] + ar
            st[rows, im] = st[rows, im] + ai
            return 0

        lax.fori_loop(0, L, settle, 0)

    y = jnp.dot(st[...].astype(BF16), read, preferred_element_type=F32)
    y = y + skip_ref[...] * xv.astype(F32)
    y = 0.5 * y * (1.0 + jnp.tanh(0.7978845608028654 * (y + 0.044715 * y * y * y)))
    heads = []
    for h in range(W // NORM_W):
        part = y[:, h * NORM_W : (h + 1) * NORM_W]
        scale = lax.rsqrt(jnp.mean(part * part, axis=1, keepdims=True) + EPSILON)
        heads.append(part * scale * gain_ref[:, h * NORM_W : (h + 1) * NORM_W])
    merged = jnp.concatenate(heads, axis=1).astype(BF16)
    t = lax.broadcasted_iota(jnp.int32, (n, n), 0)
    r = lax.broadcasted_iota(jnp.int32, (n, n), 1)
    unmix = (r == (t % L) * SUB + t // L).astype(BF16)
    mg[...] = jnp.dot(unmix, merged, preferred_element_type=F32).astype(BF16).reshape(ntp, q, W)

    def row_copy(k):
        to = lax.rem(tp + k, ntp)
        return pltpu.make_async_remote_copy(
            src_ref=mg.at[to], dst_ref=rows_in.at[k - 1],
            send_sem=s_rows.at[k - 1], recv_sem=r_rows.at[k - 1],
            device_id=(sp, to), device_id_type=MESH)

    for k in range(1, ntp):
        row_copy(k).start()
    emit_copy.wait()
    mrg[:, pl.ds(pl.multiple_of(tp * W, 128), W)] = mg[tp]
    mid_out[:, pl.ds(pl.multiple_of(tp * Dl, 128), Dl)] = resid_ref[pl.ds(pl.multiple_of(tp * q, q), q), :].astype(F32)
    for k in range(1, ntp):
        src = lax.rem(tp - k + ntp, ntp)
        res_copy(k).wait_recv()
        mid_out[:, pl.ds(pl.multiple_of(src * Dl, 128), Dl)] = resid_in[k - 1].astype(F32)
        row_copy(k).wait_recv()
        mrg[:, pl.ds(pl.multiple_of(src * W, 128), W)] = rows_in[k - 1]
    mid = mid_out[...] + jnp.dot(mrg[...], emit[...], preferred_element_type=F32)
    mid_out[...] = mid
    scale = lax.rsqrt(jnp.mean(mid * mid, axis=1, keepdims=True) + EPSILON)
    normed_out[...] = (mid * scale * lead_ref[...]).astype(BF16)
    for k in range(1, nsp):
        ends_copy(k).wait_send()
    for k in range(1, ntp):
        res_copy(k).wait_send()
        row_copy(k).wait_send()


def on_device(residual, lifted, dts, fades, long_rate, short_rate, long_freq, short_freq,
              long_lin, short_lin, skip, closing, emitted, leading, raising, lowering):
    nsp, ntp = lax.axis_size("sp"), lax.axis_size("tp")
    rank = lax.axis_index("tp")
    n, W = lifted.shape
    G = dts.shape[0]
    half = G // 2
    PL, PS = long_rate.shape[2], short_rate.shape[2]
    S = half * (PL + PS)
    D = emitted.shape[1]
    Dl = residual.shape[1]
    L, q = n // SUB, n // ntp

    def owned(array, axis, count):
        return lax.dynamic_slice_in_dim(array, rank * count, count, axis)

    x = lifted.reshape(SUB, L, W).transpose(1, 0, 2).reshape(n, W)
    mix = lambda a: a.reshape(G, SUB, L).transpose(2, 1, 0).reshape(n, G)
    flat = lambda a, b: jnp.concatenate(
        [owned(a, 1, half).reshape(2, -1), owned(b, 1, half).reshape(2, -1)], axis=1)
    rates = jnp.stack([flat(long_rate, short_rate), flat(long_freq, short_freq)], axis=1).reshape(4, S)
    lin = jnp.concatenate(
        [owned(long_lin, 3, half).reshape(8, half * PL, CHAN),
         owned(short_lin, 3, half).reshape(8, half * PS, CHAN)], axis=1)
    cfg = (nsp, ntp, n, S, W, G, PL, PS, D)
    vm = pl.BlockSpec(memory_space=pltpu.VMEM)
    dma = pltpu.SemaphoreType.DMA
    mid, normed = pl.pallas_call(
        functools.partial(mixer_body, cfg),
        out_shape=(jax.ShapeDtypeStruct((q, D), F32), jax.ShapeDtypeStruct((q, D), BF16)),
        in_specs=[vm] * 9 + [pl.BlockSpec(memory_space=pl.ANY)],
        out_specs=(vm, vm),
        scratch_shapes=[
            pltpu.VMEM((n, S), F32), pltpu.VMEM((n, S), F32),
            pltpu.VMEM((n, 4 * S), F32), pltpu.VMEM((n, 4 * S), F32),
            pltpu.VMEM((8, SUB, S), F32), pltpu.VMEM((8, S), F32), pltpu.VMEM((nsp - 1, 8, S), F32),
            pltpu.VMEM((4, SUB, S), F32),
            pltpu.VMEM((ntp, q, W), BF16), pltpu.VMEM((ntp - 1, q, W), BF16),
            pltpu.VMEM((q, ntp * W), BF16), pltpu.VMEM(emitted.shape, BF16),
            pltpu.VMEM((ntp - 1, q, Dl), BF16),
            dma((1,)), dma((nsp - 1,)), dma((nsp - 1,)), dma((ntp - 1,)), dma((ntp - 1,)),
            dma((ntp - 1,)), dma((ntp - 1,)),
        ],
        compiler_params=pltpu.CompilerParams(collective_id=0, has_side_effects=True),
        cost_estimate=pl.CostEstimate(flops=10**9, bytes_accessed=3 * 10**7, transcendentals=10**6),
    )(x, mix(dts), mix(fades), rates, lin, owned(skip, 0, W)[None], owned(closing, 0, W)[None],
      residual, leading[None], emitted)
    whole_rows = lax.all_gather(normed, "tp", axis=0, tiled=True)
    upward = jnp.dot(whole_rows, lax.all_gather(raising, "sp", axis=0, tiled=True),
                     preferred_element_type=F32)
    hidden = jnp.square(jax.nn.relu(upward)).astype(BF16)
    partial_value = jnp.dot(hidden, lax.all_gather(lowering, "sp", axis=1, tiled=True),
                            preferred_element_type=F32)
    feed = lax.psum_scatter(partial_value.astype(BF16), "tp", scatter_dimension=0, tiled=True).astype(F32)
    out = (mid + feed).astype(BF16)
    return lax.all_to_all(out, "tp", split_axis=1, concat_axis=0, tiled=True)


def solution(mesh):
    both, swapped = P("sp", "tp"), P("tp", "sp")
    in_specs = (both, both, swapped, swapped) + (P(),) * 10 + (both, swapped)
    return jax.shard_map(on_device, mesh=mesh, in_specs=in_specs, out_specs=both, check_vma=False)
```

profile of v0, /device:TPU:31, one launch (start us, length us, event | category | flops | bytes accessed | tf_op | source)
XLA Modules:
  0.0 308.2 jit_solution(14019604718385240374)
XLA Ops:
  6.5 0.7 all-gather.5.cloned.1.call-update
  7.3 0.7 all-gather.3.cloned.1.call-update
  8.0 0.0 reduce-scatter.2.cloned.1.call-start
  8.1 1.5 copy.34
  9.6 0.8 reshape.44
  10.3 0.7 copy.24
  11.0 0.8 reshape.46
  11.8 0.7 copy.25
  12.5 0.7 constant_dynamic-slice_fusion.2
  13.3 0.1 reshape.51
  13.3 0.7 constant_dynamic-slice_fusion.3
  14.0 0.1 reshape.50
  14.1 0.1 reshape.49
  14.2 0.1 reshape.48
  14.3 0.6 reshape.52.rates_ref
  15.0 1.1 constant_dynamic-slice_fusion
  16.0 0.2 copy.27
  16.2 0.2 reshape.54
  16.5 0.2 copy.26
  16.6 0.1 reshape.53
  16.8 2.2 copy.28.lin_ref
  19.0 1.3 dynamic_slice.30
  20.3 1.3 dynamic_slice.31
  21.6 29.6 %shard_map.154 = (f32[32,2048]{1,0:T(8,128)}, bf16[32,2048]{1,0:T(8,128)(2,1)}) custom-call(bf16[128,256]{1,0:T(8,128)(2,1)} %bitcast.36, f32[128,16]{1,0:T(8,128)} %bitcast.37, f32[128,16]{1,0:T(8,128)} %bitcast.38, f32[4,768]{1,0:T(4,128)} %reshape.52.rates_ref, f32[8,768,16]{2,1,0:T(8,128)} %copy.28.lin_ref, f32[1,256]{1,0:T(1,128)} %bitcast.41, ...), custom_call_target="tpu_custom_call" | custom-call | flops 1000000000 | bytes 30000000 | tf_op jit(solution)/shard_map/pallas_call | solution.py:260
  51.3 7.5 %all_gather.9 = bf16[128,2048]{1,0:T(8,128)(2,1)S(1)} all-gather(bf16[32,2048]{1,0:T(8,128)(2,1)} %get-tuple-element.8), channel_id=1, replica_groups=mesh['sp'=8,'tp'=4] {'tp'}, dimensions={0}, use_global_device_ids=true | all-gather | bytes 655360 | tf_op jit(solution)/shard_map/all_gather | solution.py:280
  58.8 78.8 %all-gather.5.cloned.1.call-done = bf16[2048,2048]{1,0:T(8,128)(2,1)} async-done(((bf16[2048,256]{1,0:T(8,128)(2,1)}), bf16[2048,2048]{1,0:T(8,128)(2,1)}) %all-gather.5.cloned.1.call-update) | async-done | bytes 8388624 | tf_op jit(solution)/shard_map/all_gather | solution.py:284
  137.5 124.8 %all-gather.3.cloned.1.call-done = bf16[2048,2048]{1,0:T(8,128)(2,1)} async-done(((bf16[256,2048]{1,0:T(8,128)(2,1)}), bf16[2048,2048]{1,0:T(8,128)(2,1)}) %all-gather.3.cloned.1.call-update) | async-done | bytes 8388624 | tf_op jit(solution)/shard_map/all_gather | solution.py:281
  262.3 8.9 %convolution_convert_fusion = bf16[128,2048]{1,0:T(8,128)(2,1)} fusion(bf16[2048,2048]{1,0:T(8,128)(2,1)} %all-gather.5.cloned.1.call-done, bf16[128,2048]{1,0:T(8,128)(2,1)S(1)} %all_gather.9, bf16[2048,2048]{1,0:T(8,128)(2,1)} %all-gather.3.cloned.1.call-done), kind=kOutput, calls=%fused_computation.2 | convolution fusion | flops 2148532224 | bytes 17825792 | tf_op jit(solution)/shard_map/dot_general | solution.py:284
  271.3 21.7 %reduce-scatter.2.cloned.1.call-done = bf16[32,2048]{1,0:T(8,128)(2,1)} async-done(((bf16[128,2048]{1,0:T(8,128)(2,1)}), bf16[32,2048]{1,0:T(8,128)(2,1)}) %reduce-scatter.2.cloned.1.call-update) | async-done | bytes 131088 | tf_op jit(solution)/shard_map/reduce_scatter | solution.py:286
  293.0 0.9 add_convert_fusion
  293.9 7.1 %all_to_all.19 = bf16[32,4,512]{2,0,1:T(8,128)(2,1)S(1)} all-to-all(bf16[32,4,512]{2,0,1:T(8,128)(2,1)S(1)} %bitcast.33), channel_id=1, replica_groups=mesh['sp'=8,'tp'=4] {'tp'}, dimensions={1} | all-to-all | bytes 262144 | tf_op jit(solution)/shard_map/all_to_all | solution.py:288
  301.0 0.7 copy.36
  (15 shorter events, 0.2 us)
Async XLA Ops:
  6.5 9.9 %copy-start = (f32[2,2,2,32,64,16]{4,5,3,2,1,0:T(8,128)S(1)}, f32[2,2,2,32,64,16]{4,5,3,2,1,0:T(8,128)}, u32[]{:S(2)}) copy-start(f32[2,2,2,32,64,16]{4,5,3,2,1,0:T(8,128)} %param.24) | copy-start | bytes 3145732
  6.5 131.0 %all-gather.5.cloned.1.call-start = ((), (), s32[]{:S(2)}) async-start(), calls=%async_computation.3 | async-start | bytes 9437184 | tf_op jit(solution)/shard_map/all_gather | solution.py:284
  7.3 255.1 %all-gather.3.cloned.1.call-start = ((), (), s32[]{:S(2)}) async-start(), calls=%async_computation.2 | async-start | bytes 9437184 | tf_op jit(solution)/shard_map/all_gather | solution.py:281
  8.0 285.0 %reduce-scatter.2.cloned.1.call-start = ((), (), s32[]{:S(2)}) async-start(), calls=%async_computation.4 | async-start | bytes 655360 | tf_op jit(solution)/shard_map/reduce_scatter | solution.py:286
  58.8 234.2 %copy-start.1 = (f32[32,2048]{1,0:T(8,128)S(1)}, f32[32,2048]{1,0:T(8,128)}, u32[]{:S(2)}) copy-start(f32[32,2048]{1,0:T(8,128)} %get-tuple-element.7) | copy-start | bytes 786436
Sparse Core Ops, SparseCore 0:
  9.4 128.1 all-gather.4
  139.7 122.6 all-gather.2
  271.4 21.5 reduce-scatter.1
where the time goes:
time: 311 us; the launch traced here: 308 us
  waiting for transfers between devices  227 us (73%)
  Pallas kernels  29.6 us (10%)
  blocking collectives  14.5 us (5%)
  local copies, waits for them, and re-layouts  14.1 us (5%)
  between operations  13.2 us (4%)
  matrix products  8.93 us (3%)
    all_gather x1, waiting for transfers between devices, on_device(): lax.all_gather(raising, 'sp', axis=0, tiled=True)  125 us
    all_gather x1, waiting for transfers between devices, on_device(): lax.all_gather(lowering, 'sp', axis=1, tiled=True)  78.8 us
    pallas_call x1, Pallas kernels, on_device(): pl.pallas_call(functools.partial(mixer_body, cfg), out_shape=(jax.ShapeDt...  29.6 us
    reduce_scatter x1, waiting for transfers between devices, on_device(): lax.psum_scatter(partial_value.astype(BF16), 'tp', scatter_dimension=0, t...  21.7 us
    dot_general x1, matrix products, on_device(): jnp.dot(hidden, lax.all_gather(lowering, 'sp', axis=1, tiled=True), prefe...  8.93 us
    all_gather x1, blocking collectives, on_device(): whole_rows = lax.all_gather(normed, 'tp', axis=0, tiled=True)  7.49 us
    all_to_all x1, blocking collectives, on_device(): return lax.all_to_all(out, 'tp', split_axis=1, concat_axis=0, tiled=True)  7.06 us
  transfers between devices with their start and end apart: 3, of which 3 were waited for; matrix products, arithmetic and copies ran while one was open for 4% of the time, Pallas kernels for 10%

commit v1 on v0

--- a/solution.py
+++ b/solution.py
@@ -44,10 +44,14 @@
 
 
 def mixer_body(cfg, x_ref, dt_ref, lf_ref, rates_ref, lin_ref, skip_ref, gain_ref,
-               resid_ref, lead_ref, emit_hbm, mid_out, normed_out,
+               resid_ref, lead_ref, emit_hbm, up_hbm, down_hbm, out_ref,
                pace, surge, pre, st, blk, ends, ends_all, cin, mg, rows_in, mrg, emit, resid_in,
-               copy_sem, s_ends, r_ends, s_rows, r_rows, s_res, r_res):
-    nsp, ntp, n, S, W, G, PL, PS, D = cfg
+               mid_out, wup, wdn, nrm, hid, part, rs_in, fin, fin_in,
+               copy_sem, s_ends, r_ends, s_rows, r_rows, s_res, r_res,
+               s_u1, r_u1, s_d1, r_d1, s_u2, r_u2, s_d2, r_d2, s_u3, r_u3, s_d3, r_d3,
+               s_nrm, r_nrm, s_rs, r_rs, s_fin, r_fin):
+    nsp, ntp, n, S, W, G, PL, PS, D, c_ff, F = cfg
+    M = ntp // 2
     L = n // SUB
     half = G // 2
     SL = half * PL
@@ -59,6 +63,48 @@
 
     emit_copy = pltpu.make_async_copy(emit_hbm, emit, copy_sem.at[0])
     emit_copy.start()
+    chunk = lax.rem(sp, c_ff)
+    partner = tp + 1 - 2 * lax.rem(tp, 2)
+
+    def cols(of):
+        return pl.ds(pl.multiple_of(of * F, 128), F)
+
+    own_up = pltpu.make_async_copy(up_hbm.at[:, cols(chunk)], wup.at[tp, sp], copy_sem.at[1])
+    own_down = pltpu.make_async_copy(down_hbm.at[cols(chunk), :], wdn.at[tp, sp], copy_sem.at[2])
+    own_up.start()
+    own_down.start()
+
+    def spread_copy(k, up):
+        to = lax.rem(sp + k, nsp)
+        src = up_hbm.at[:, cols(lax.rem(to, c_ff))] if up else down_hbm.at[cols(lax.rem(to, c_ff)), :]
+        return pltpu.make_async_remote_copy(
+            src_ref=src, dst_ref=(wup if up else wdn).at[tp, sp],
+            send_sem=(s_u1 if up else s_d1).at[k - 1], recv_sem=(r_u1 if up else r_d1).at[k - 1],
+            device_id=(to, tp), device_id_type=MESH)
+
+    def across_copy(m, k, up):
+        piece = (wup if up else wdn).at[tp, lax.rem(sp - k + nsp, nsp)]
+        return pltpu.make_async_remote_copy(
+            src_ref=piece, dst_ref=piece,
+            send_sem=(s_u2 if up else s_d2).at[m - 1, k], recv_sem=(r_u2 if up else r_d2).at[m - 1, k],
+            device_id=(sp, lax.rem(tp + 2 * m, ntp)), device_id_type=MESH)
+
+    def pair_copy(m, up):
+        piece = (wup if up else wdn).at[lax.rem(tp + 2 * m, ntp)]
+        return pltpu.make_async_remote_copy(
+            src_ref=piece, dst_ref=piece,
+            send_sem=(s_u3 if up else s_d3).at[m], recv_sem=(r_u3 if up else r_d3).at[m],
+            device_id=(sp, partner), device_id_type=MESH)
+
+    def pass_on(first, last, up):
+        for k in range(first, last):
+            if k == 0:
+                (own_up if up else own_down).wait()
+            else:
+                spread_copy(k, up).wait_recv()
+            for m in range(1, M):
+                across_copy(m, k, up).start()
+
     barrier = pltpu.get_barrier_semaphore()
     for k in range(1, nsp):
         pl.semaphore_signal(barrier, inc=1, device_id=(lax.rem(sp + k, nsp), tp), device_id_type=MESH)
@@ -73,6 +119,8 @@
             send_sem=s_res.at[k - 1], recv_sem=r_res.at[k - 1],
             device_id=(sp, to), device_id_type=MESH)
 
+    for k in range(1, nsp):
+        spread_copy(k, True).start()
     for k in range(1, ntp):
         res_copy(k).start()
 
@@ -147,10 +195,13 @@
 
     for k in range(1, nsp):
         ends_copy(k).start()
+    for k in range(1, nsp):
+        spread_copy(k, False).start()
 
     read = jnp.concatenate(
         [block_map(2), block_map(3, -1.0), block_map(6), block_map(7, -1.0)], axis=0)
 
+    pass_on(0, nsp // 2, True)
     for k in range(1, nsp):
         ends_copy(k).wait_recv()
     blank = jnp.zeros((1, S), F32)
@@ -192,9 +243,9 @@
     y = 0.5 * y * (1.0 + jnp.tanh(0.7978845608028654 * (y + 0.044715 * y * y * y)))
     heads = []
     for h in range(W // NORM_W):
-        part = y[:, h * NORM_W : (h + 1) * NORM_W]
-        scale = lax.rsqrt(jnp.mean(part * part, axis=1, keepdims=True) + EPSILON)
-        heads.append(part * scale * gain_ref[:, h * NORM_W : (h + 1) * NORM_W])
+        head = y[:, h * NORM_W : (h + 1) * NORM_W]
+        scale = lax.rsqrt(jnp.mean(head * head, axis=1, keepdims=True) + EPSILON)
+        heads.append(head * scale * gain_ref[:, h * NORM_W : (h + 1) * NORM_W])
     merged = jnp.concatenate(heads, axis=1).astype(BF16)
     t = lax.broadcasted_iota(jnp.int32, (n, n), 0)
     r = lax.broadcasted_iota(jnp.int32, (n, n), 1)
@@ -210,6 +261,7 @@
 
     for k in range(1, ntp):
         row_copy(k).start()
+    pass_on(nsp // 2, nsp, True)
     emit_copy.wait()
     mrg[:, pl.ds(pl.multiple_of(tp * W, 128), W)] = mg[tp]
     mid_out[:, pl.ds(pl.multiple_of(tp * Dl, 128), Dl)] = resid_ref[pl.ds(pl.multiple_of(tp * q, q), q), :].astype(F32)
@@ -222,7 +274,91 @@
     mid = mid_out[...] + jnp.dot(mrg[...], emit[...], preferred_element_type=F32)
     mid_out[...] = mid
     scale = lax.rsqrt(jnp.mean(mid * mid, axis=1, keepdims=True) + EPSILON)
-    normed_out[...] = (mid * scale * lead_ref[...]).astype(BF16)
+    base, q_all = sp - chunk, c_ff * q
+    nrm[chunk] = (mid * scale * lead_ref[...]).astype(BF16)
+
+    def peer(k):
+        return lax.rem(chunk + k, c_ff)
+
+    def nrm_copy(k):
+        return pltpu.make_async_remote_copy(
+            src_ref=nrm.at[chunk], dst_ref=nrm.at[chunk],
+            send_sem=s_nrm.at[k - 1], recv_sem=r_nrm.at[k - 1],
+            device_id=(base + peer(k), tp), device_id_type=MESH)
+
+    def rs_copy(k):
+        return pltpu.make_async_remote_copy(
+            src_ref=part.at[peer(k)], dst_ref=rs_in.at[k - 1],
+            send_sem=s_rs.at[k - 1], recv_sem=r_rs.at[k - 1],
+            device_id=(base + peer(k), tp), device_id_type=MESH)
+
+    def fin_copy(k):
+        to = lax.rem(tp + k, ntp)
+        return pltpu.make_async_remote_copy(
+            src_ref=fin.at[to], dst_ref=fin_in.at[k - 1],
+            send_sem=s_fin.at[k - 1], recv_sem=r_fin.at[k - 1],
+            device_id=(sp, to), device_id_type=MESH)
+
+    for k in range(1, c_ff):
+        nrm_copy(k).start()
+    pair_copy(0, True).start()
+    pass_on(0, nsp, False)
+    pair_copy(0, False).start()
+    for up in (True, False):
+        for m in range(1, M):
+            for k in range(nsp):
+                across_copy(m, k, up).wait_recv()
+            pair_copy(M - m, up).start()
+        if up:
+            for m in range(M):
+                pair_copy(m, True).wait_recv()
+            for k in range(1, c_ff):
+                nrm_copy(k).wait_recv()
+            rows = nrm[...].reshape(q_all, D)
+
+            def raise_step(t, _):
+                upward = jnp.dot(rows, wup[t].reshape(D, F), preferred_element_type=F32)
+                hid[t] = jnp.square(jnp.maximum(upward, 0.0)).astype(BF16)
+                return 0
+
+            lax.fori_loop(0, ntp, raise_step, 0)
+    for m in range(M):
+        pair_copy(m, False).wait_recv()
+    Dc = D // nsp
+    for j in range(nsp):
+        total = jnp.dot(hid[0], wdn[0, j], preferred_element_type=F32)
+        for t in range(1, ntp):
+            total = total + jnp.dot(hid[t], wdn[t, j], preferred_element_type=F32)
+        part[:, :, j * Dc : (j + 1) * Dc] = total.astype(BF16).reshape(c_ff, q, Dc)
+    for k in range(1, c_ff):
+        rs_copy(k).start()
+    result = mid_out[...] + part[chunk].astype(F32)
+    for k in range(1, c_ff):
+        rs_copy(k).wait_recv()
+        result = result + rs_in[k - 1].astype(F32)
+    result = result.astype(BF16)
+    for t in range(ntp):
+        fin[t] = result[:, t * Dl : (t + 1) * Dl]
+    for k in range(1, ntp):
+        fin_copy(k).start()
+    out_ref[pl.ds(pl.multiple_of(tp * q, q), q), :] = fin[tp]
+    for k in range(1, ntp):
+        fin_copy(k).wait_recv()
+        src = lax.rem(tp - k + ntp, ntp)
+        out_ref[pl.ds(pl.multiple_of(src * q, q), q), :] = fin_in[k - 1]
+    for k in range(1, c_ff):
+        nrm_copy(k).wait_send()
+        rs_copy(k).wait_send()
+    for k in range(1, ntp):
+        fin_copy(k).wait_send()
+    for up in (True, False):
+        for k in range(1, nsp):
+            spread_copy(k, up).wait_send()
+        for m in range(1, M):
+            for k in range(nsp):
+                across_copy(m, k, up).wait_send()
+        for m in range(M):
+            pair_copy(m, up).wait_send()
     for k in range(1, nsp):
         ends_copy(k).wait_send()
     for k in range(1, ntp):
@@ -254,14 +390,17 @@
     lin = jnp.concatenate(
         [owned(long_lin, 3, half).reshape(8, half * PL, CHAN),
          owned(short_lin, 3, half).reshape(8, half * PS, CHAN)], axis=1)
-    cfg = (nsp, ntp, n, S, W, G, PL, PS, D)
+    c_ff = min(nsp, raising.shape[1] // 128)
+    F = raising.shape[1] // c_ff
+    q_all, M = c_ff * q, ntp // 2
+    cfg = (nsp, ntp, n, S, W, G, PL, PS, D, c_ff, F)
     vm = pl.BlockSpec(memory_space=pltpu.VMEM)
     dma = pltpu.SemaphoreType.DMA
-    mid, normed = pl.pallas_call(
+    return pl.pallas_call(
         functools.partial(mixer_body, cfg),
-        out_shape=(jax.ShapeDtypeStruct((q, D), F32), jax.ShapeDtypeStruct((q, D), BF16)),
-        in_specs=[vm] * 9 + [pl.BlockSpec(memory_space=pl.ANY)],
-        out_specs=(vm, vm),
+        out_shape=jax.ShapeDtypeStruct((n, Dl), BF16),
+        in_specs=[vm] * 9 + [pl.BlockSpec(memory_space=pl.ANY)] * 3,
+        out_specs=vm,
         scratch_shapes=[
             pltpu.VMEM((n, S), F32), pltpu.VMEM((n, S), F32),
             pltpu.VMEM((n, 4 * S), F32), pltpu.VMEM((n, 4 * S), F32),
@@ -270,22 +409,20 @@
             pltpu.VMEM((ntp, q, W), BF16), pltpu.VMEM((ntp - 1, q, W), BF16),
             pltpu.VMEM((q, ntp * W), BF16), pltpu.VMEM(emitted.shape, BF16),
             pltpu.VMEM((ntp - 1, q, Dl), BF16),
-            dma((1,)), dma((nsp - 1,)), dma((nsp - 1,)), dma((ntp - 1,)), dma((ntp - 1,)),
+            pltpu.VMEM((q, D), F32),
+            pltpu.VMEM((ntp, nsp, D // nsp, F), BF16), pltpu.VMEM((ntp, nsp, F, D // nsp), BF16),
+            pltpu.VMEM((c_ff, q, D), BF16), pltpu.VMEM((ntp, q_all, F), BF16),
+            pltpu.VMEM((c_ff, q, D), BF16), pltpu.VMEM((c_ff - 1, q, D), BF16),
+            pltpu.VMEM((ntp, q, Dl), BF16), pltpu.VMEM((ntp - 1, q, Dl), BF16),
+            dma((3,)), dma((nsp - 1,)), dma((nsp - 1,)), dma((ntp - 1,)), dma((ntp - 1,)),
             dma((ntp - 1,)), dma((ntp - 1,)),
+            *[dma((nsp - 1,))] * 4, *[dma((M - 1, nsp))] * 4, *[dma((M,))] * 4,
+            *[dma((c_ff - 1,))] * 4, *[dma((ntp - 1,))] * 2,
         ],
         compiler_params=pltpu.CompilerParams(collective_id=0, has_side_effects=True),
         cost_estimate=pl.CostEstimate(flops=10**9, bytes_accessed=3 * 10**7, transcendentals=10**6),
     )(x, mix(dts), mix(fades), rates, lin, owned(skip, 0, W)[None], owned(closing, 0, W)[None],
-      residual, leading[None], emitted)
-    whole_rows = lax.all_gather(normed, "tp", axis=0, tiled=True)
-    upward = jnp.dot(whole_rows, lax.all_gather(raising, "sp", axis=0, tiled=True),
-                     preferred_element_type=F32)
-    hidden = jnp.square(jax.nn.relu(upward)).astype(BF16)
-    partial_value = jnp.dot(hidden, lax.all_gather(lowering, "sp", axis=1, tiled=True),
-                            preferred_element_type=F32)
-    feed = lax.psum_scatter(partial_value.astype(BF16), "tp", scatter_dimension=0, tiled=True).astype(F32)
-    out = (mid + feed).astype(BF16)
-    return lax.all_to_all(out, "tp", split_axis=1, concat_axis=0, tiled=True)
+      residual, leading[None], emitted, raising, lowering)
 
 
 def solution(mesh):

time: 311 us -> 128 us (0.41)
  waiting for transfers between devices: 227 us -> 0 us
  Pallas kernels: 29.6 us -> 115 us
  blocking collectives: 14.5 us -> 0 us
  between operations: 13.2 us -> 0.11 us
  matrix products: 8.93 us -> 0 us
    all_gather x2 -> x0, waiting for transfers between devices: 204 us -> none  [the longest x1 125 us: on_device(): lax.all_gather(raising, 'sp', axis=0, tiled=True)]
    pallas_call x1, Pallas kernels: 29.6 us -> 115 us  [on_device(): pl.pallas_call(functools.partial(mixer_body, cfg), out_shape=jax.ShapeDty...]
    reduce_scatter x1 -> x0, waiting for transfers between devices: 21.7 us -> none  [on_device(): lax.psum_scatter(partial_value.astype(BF16), 'tp', scatter_dimension=0, t...]
    dot_general x1 -> x0, matrix products: 8.93 us -> none  [on_device(): jnp.dot(hidden, lax.all_gather(lowering, 'sp', axis=1, tiled=True), prefe...]
    all_gather x1 -> x0, blocking collectives: 7.49 us -> none  [on_device(): whole_rows = lax.all_gather(normed, 'tp', axis=0, tiled=True)]
    all_to_all x1 -> x0, blocking collectives: 7.06 us -> none  [on_device(): return lax.all_to_all(out, 'tp', split_axis=1, concat_axis=0, tiled=True)]
  transfers between devices with their start and end apart: 3 -> 0, of which waited for: 3 -> 0; matrix products, arithmetic and copies ran while one was open for 4% -> 0% of each run, Pallas kernels for 10% -> 0%
where the time goes in v1:
time: 128 us
  Pallas kernels  115 us (90%)
  local copies, waits for them, and re-layouts  12.9 us (10%)
    pallas_call x1, Pallas kernels, on_device(): pl.pallas_call(functools.partial(mixer_body, cfg), out_shape=jax.ShapeDty...  115 us
    dynamic_slice x8, local copies, waits for them, and re-layouts, owned(): return lax.dynamic_slice_in_dim(array, rank * count, count, axis)  5.59 us

profile of v1, /device:TPU:31, one launch (start us, length us, event | category | flops | bytes accessed | tf_op | source)
XLA Modules:
  0.0 127.8 jit_solution(11272808172610174102)
XLA Ops:
  0.0 0.0 copy-start
  0.0 0.9 constant_dynamic-slice_fusion.3
  0.9 0.1 reshape.47
  0.9 0.7 constant_dynamic-slice_fusion.2
  1.7 0.1 reshape.48
  1.8 0.1 reshape.45
  1.8 0.1 reshape.46
  2.0 0.6 reshape.49.rates_ref
  2.6 0.0 copy-done
  2.6 0.2 copy.25
  2.8 0.1 reshape.50
  2.9 1.1 constant_dynamic-slice_fusion
  4.0 0.2 copy.26
  4.2 0.2 reshape.51
  4.4 0.0 copy-start.2
  4.4 0.0 copy-start.3
  4.4 0.0 copy-start.1
  4.4 2.2 %copy.27.lin_ref = f32[8,768,16]{2,1,0:T(8,128)} copy(f32[8,768,16]{1,2,0:T(8,128)S(1)} %pad_maximum_fusion) | data formatting | bytes 786432 | tf_op jit(solution)/shard_map/concatenate | solution.py:390
  6.6 1.3 %dynamic_slice.30 = f32[256]{0:T(256)} dynamic-slice(f32[1024]{0:T(1024)} %param.26, s32[]{:T(128)S(6)} %select_n.5), dynamic_slice_sizes={256} | dynamic-slice | bytes 2052 | tf_op jit(solution)/shard_map/dynamic_slice | solution.py:383
  7.9 1.3 dynamic_slice.31
  9.2 0.0 copy-done.2
  9.2 0.1 reshape.41
  9.3 0.7 copy.23
  10.0 0.0 copy-done.3
  10.0 0.1 reshape.43
  10.1 0.7 copy.24
  10.8 0.0 copy-done.1
  10.8 0.7 copy.29
  11.5 114.8 %shard_map.154 = bf16[128,512]{1,0:T(8,128)(2,1)} custom-call(bf16[128,256]{1,0:T(8,128)(2,1)} %bitcast.25, f32[128,16]{1,0:T(8,128)} %bitcast.23, f32[128,16]{1,0:T(8,128)} %bitcast.24, f32[4,768]{1,0:T(4,128)} %reshape.49.rates_ref, f32[8,768,16]{2,1,0:T(8,128)} %copy.27.lin_ref, f32[1,256]{1,0:T(1,128)} %bitcast.28, f32[1,256]{1,0:T(1,128)} %bitcast.29, ...), custom_call_target="tpu_custom_call" | custom-call | flops 1000000000 | bytes 30000000 | tf_op jit(solution)/shard_map/pallas_call | solution.py:399
  126.3 1.6 %copy.31 = bf16[128,512]{1,0:T(8,128)(2,1)} copy(bf16[128,512]{1,0:T(8,128)(2,1)} %shard_map.154) | data formatting | bytes 262144
  (7 shorter events, 0.1 us)
Async XLA Ops:
  0.0 2.6 %copy-start = (f32[2,2,2,32,64,16]{4,5,3,2,1,0:T(8,128)S(1)}, f32[2,2,2,32,64,16]{4,5,3,2,1,0:T(8,128)}, u32[]{:S(2)}) copy-start(f32[2,2,2,32,64,16]{4,5,3,2,1,0:T(8,128)} %param.24) | copy-start | bytes 3145732
  4.4 4.8 %copy-start.2 = (f32[16,128]{1,0:T(8,128)S(1)}, f32[16,128]{1,0:T(8,128)}, u32[]{:S(2)}) copy-start(f32[16,128]{1,0:T(8,128)} %param.18) | copy-start | bytes 24580
  4.4 5.6 %copy-start.3 = (f32[16,128]{1,0:T(8,128)S(1)}, f32[16,128]{1,0:T(8,128)}, u32[]{:S(2)}) copy-start(f32[16,128]{1,0:T(8,128)} %param.19) | copy-start | bytes 24580
  4.4 6.4 %copy-start.1 = (bf16[128,256]{1,0:T(8,128)(2,1)S(1)}, bf16[128,256]{1,0:T(8,128)(2,1)}, u32[]{:S(2)}) copy-start(bf16[128,256]{1,0:T(8,128)(2,1)} %param.17) | copy-start | bytes 196612

commit v2 on v1

--- a/solution.py
+++ b/solution.py
@@ -43,8 +43,9 @@
     return ar * br - ai * bi, ar * bi + ai * br
 
 
-def mixer_body(cfg, x_ref, dt_ref, lf_ref, rates_ref, lin_ref, skip_ref, gain_ref,
-               resid_ref, lead_ref, emit_hbm, up_hbm, down_hbm, out_ref,
+def mixer_body(cfg, x_ref, dt_ref, lf_ref, long_rate, short_rate, long_freq, short_freq,
+               skip_ref, gain_ref, resid_ref, lead_ref, long_hbm, short_hbm, emit_hbm, up_hbm, down_hbm,
+               out_ref, lin_l, lin_s, lin_sem,
                pace, surge, pre, st, blk, ends, ends_all, cin, mg, rows_in, mrg, emit, resid_in,
                mid_out, wup, wdn, nrm, hid, part, rs_in, fin, fin_in,
                copy_sem, s_ends, r_ends, s_rows, r_rows, s_res, r_res,
@@ -62,6 +63,14 @@
     MESH = pl.DeviceIdType.MESH
 
     emit_copy = pltpu.make_async_copy(emit_hbm, emit, copy_sem.at[0])
+    lin_copies = []
+    for at in range(8):
+        for kind, (src, dst) in enumerate(((long_hbm, lin_l), (short_hbm, lin_s))):
+            lin_copies.append(pltpu.make_async_copy(
+                src.at[at // 4, at // 2 % 2, at % 2, pl.ds(tp * half, half)], dst.at[at],
+                lin_sem.at[kind, at]))
+    for copy in lin_copies:
+        copy.start()
     emit_copy.start()
     chunk = lax.rem(sp, c_ff)
     partner = tp + 1 - 2 * lax.rem(tp, 2)
@@ -127,28 +136,63 @@
     lane = lax.broadcasted_iota(jnp.int32, (G, S), 1)
     group = jnp.where(lane < SL, 2 * (lane // PL), 2 * ((lane - SL) // PS) + 1)
     spread = (group == lax.broadcasted_iota(jnp.int32, (G, S), 0)).astype(F32)
-    pace[...] = jnp.dot(dt_ref[...], spread, precision=lax.Precision.HIGHEST, preferred_element_type=F32)
-    surge[...] = jnp.dot(lf_ref[...], spread, precision=lax.Precision.HIGHEST, preferred_element_type=F32)
-
-    row = lax.broadcasted_iota(jnp.int32, (S, W), 0)
-    row_group = jnp.where(row < SL, 2 * (row // PL), 2 * ((row - SL) // PS) + 1)
-    mask = row_group == lax.broadcasted_iota(jnp.int32, (S, W), 1) // CHAN
-    tile = (lax.broadcasted_iota(jnp.int32, (CHAN, W), 1) % CHAN
-            == lax.broadcasted_iota(jnp.int32, (CHAN, W), 0)).astype(BF16)
+    r = lax.broadcasted_iota(jnp.int32, (n, n), 0)
+    t = lax.broadcasted_iota(jnp.int32, (n, n), 1)
+    mix = (t == (r % SUB) * L + r // SUB).astype(F32)
+
+    def per_state(ref):
+        moved = lax.dot_general(ref[...], mix, (((1,), (1,)), ((), ())),
+                                precision=lax.Precision.HIGHEST, preferred_element_type=F32)
+        return lax.dot_general(moved, spread, (((0,), (0,)), ((), ())),
+                               precision=lax.Precision.HIGHEST, preferred_element_type=F32)
+
+    pace[...] = per_state(dt_ref)
+    surge[...] = per_state(lf_ref)
+
+    def flat_kind(ref, e):
+        many, states = ref.shape[1:]
+        width = half * states
+        repeat = (lax.broadcasted_iota(jnp.int32, (states, width), 1) % states
+                  == lax.broadcasted_iota(jnp.int32, (states, width), 0)).astype(F32)
+        wide = jnp.dot(ref[e], repeat, precision=lax.Precision.HIGHEST, preferred_element_type=F32)
+        owner = tp * half + lax.broadcasted_iota(jnp.int32, (many, width), 1) // states
+        mine = owner == lax.broadcasted_iota(jnp.int32, (many, width), 0)
+        return jnp.sum(jnp.where(mine, wide, 0.0), axis=0, keepdims=True)
+
+    def flat(long_ref, short_ref, e):
+        return jnp.concatenate([flat_kind(long_ref, e), flat_kind(short_ref, e)], axis=1)
+
+    def widened(ref, index, states, sign):
+        rows, width = half * CHAN, half * states
+        repeat = (lax.broadcasted_iota(jnp.int32, (states, width), 1) % states
+                  == lax.broadcasted_iota(jnp.int32, (states, width), 0)).astype(BF16)
+        wide = jnp.dot(ref[index].reshape(rows, states).astype(BF16), repeat, preferred_element_type=F32)
+        own_block = (lax.broadcasted_iota(jnp.int32, (rows, width), 0) // CHAN
+                     == lax.broadcasted_iota(jnp.int32, (rows, width), 1) // states)
+        return jnp.where(own_block, sign * wide, 0.0).astype(BF16)
 
     def block_map(index, sign=1.0):
-        wide = jnp.dot(lin_ref[index].astype(BF16), tile, preferred_element_type=F32)
-        return jnp.where(mask, sign * wide, 0.0).astype(BF16)
-
-    xv = x_ref[...]
+        long_part = widened(lin_l, index, PL, sign)
+        short_part = widened(lin_s, index, PS, sign)
+        no_long, no_short = jnp.zeros((CHAN, SL), BF16), jnp.zeros((CHAN, S - SL), BF16)
+        bands = []
+        for g in range(half):
+            band = slice(g * CHAN, (g + 1) * CHAN)
+            bands.append(jnp.concatenate([long_part[band], no_short], axis=1))
+            bands.append(jnp.concatenate([no_long, short_part[band]], axis=1))
+        return jnp.concatenate(bands, axis=0)
+
+    xv = jnp.dot(mix.astype(BF16), x_ref[...], preferred_element_type=F32).astype(BF16)
+    for copy in lin_copies:
+        copy.wait()
     for e in range(2):
         for c in range(2):
-            st[:, pl.ds((2 * e + c) * S, S)] = lax.dot_general(
-                xv, block_map(4 * e + c), (((1,), (1,)), ((), ())), preferred_element_type=F32)
+            st[:, pl.ds((2 * e + c) * S, S)] = jnp.dot(
+                xv, block_map(4 * e + c), preferred_element_type=F32)
 
     for e in range(2):
-        rate = rates_ref[2 * e : 2 * e + 1, :]
-        freq = rates_ref[2 * e + 1 : 2 * e + 2, :]
+        rate = flat(long_rate, short_rate, e)
+        freq = flat(long_freq, short_freq, e)
 
         def step(i, carry):
             pr, pi, sr, si = carry
@@ -199,7 +243,7 @@
         spread_copy(k, False).start()
 
     read = jnp.concatenate(
-        [block_map(2), block_map(3, -1.0), block_map(6), block_map(7, -1.0)], axis=0)
+        [block_map(2), block_map(3, -1.0), block_map(6), block_map(7, -1.0)], axis=1)
 
     pass_on(0, nsp // 2, True)
     for k in range(1, nsp):
@@ -238,14 +282,17 @@
 
         lax.fori_loop(0, L, settle, 0)
 
-    y = jnp.dot(st[...].astype(BF16), read, preferred_element_type=F32)
-    y = y + skip_ref[...] * xv.astype(F32)
+    y = lax.dot_general(st[...].astype(BF16), read, (((1,), (1,)), ((), ())),
+                        preferred_element_type=F32)
+    own = pl.ds(pl.multiple_of(tp * W, 128), W)
+    skip_row, gain_row = skip_ref[:, own], gain_ref[:, own]
+    y = y + skip_row * xv.astype(F32)
     y = 0.5 * y * (1.0 + jnp.tanh(0.7978845608028654 * (y + 0.044715 * y * y * y)))
     heads = []
     for h in range(W // NORM_W):
         head = y[:, h * NORM_W : (h + 1) * NORM_W]
         scale = lax.rsqrt(jnp.mean(head * head, axis=1, keepdims=True) + EPSILON)
-        heads.append(head * scale * gain_ref[:, h * NORM_W : (h + 1) * NORM_W])
+        heads.append(head * scale * gain_row[:, h * NORM_W : (h + 1) * NORM_W])
     merged = jnp.concatenate(heads, axis=1).astype(BF16)
     t = lax.broadcasted_iota(jnp.int32, (n, n), 0)
     r = lax.broadcasted_iota(jnp.int32, (n, n), 1)
@@ -280,11 +327,19 @@
     def peer(k):
         return lax.rem(chunk + k, c_ff)
 
-    def nrm_copy(k):
+    H = c_ff // 2
+
+    def nrm_across(m):
         return pltpu.make_async_remote_copy(
             src_ref=nrm.at[chunk], dst_ref=nrm.at[chunk],
-            send_sem=s_nrm.at[k - 1], recv_sem=r_nrm.at[k - 1],
-            device_id=(base + peer(k), tp), device_id_type=MESH)
+            send_sem=s_nrm.at[0, m], recv_sem=r_nrm.at[0, m],
+            device_id=(base + peer(2 * m), tp), device_id_type=MESH)
+
+    def nrm_pair(m):
+        return pltpu.make_async_remote_copy(
+            src_ref=nrm.at[peer(2 * m)], dst_ref=nrm.at[peer(2 * m)],
+            send_sem=s_nrm.at[1, m], recv_sem=r_nrm.at[1, m],
+            device_id=(base + chunk + 1 - 2 * lax.rem(chunk, 2), tp), device_id_type=MESH)
 
     def rs_copy(k):
         return pltpu.make_async_remote_copy(
@@ -299,11 +354,15 @@
             send_sem=s_fin.at[k - 1], recv_sem=r_fin.at[k - 1],
             device_id=(sp, to), device_id_type=MESH)
 
-    for k in range(1, c_ff):
-        nrm_copy(k).start()
+    for m in range(1, H):
+        nrm_across(m).start()
+    nrm_pair(0).start()
     pair_copy(0, True).start()
     pass_on(0, nsp, False)
     pair_copy(0, False).start()
+    for m in range(1, H):
+        nrm_across(m).wait_recv()
+        nrm_pair(H - m).start()
     for up in (True, False):
         for m in range(1, M):
             for k in range(nsp):
@@ -312,8 +371,8 @@
         if up:
             for m in range(M):
                 pair_copy(m, True).wait_recv()
-            for k in range(1, c_ff):
-                nrm_copy(k).wait_recv()
+            for m in range(H):
+                nrm_pair(m).wait_recv()
             rows = nrm[...].reshape(q_all, D)
 
             def raise_step(t, _):
@@ -347,8 +406,11 @@
         src = lax.rem(tp - k + ntp, ntp)
         out_ref[pl.ds(pl.multiple_of(src * q, q), q), :] = fin_in[k - 1]
     for k in range(1, c_ff):
-        nrm_copy(k).wait_send()
         rs_copy(k).wait_send()
+    for m in range(H):
+        if m > 0:
+            nrm_across(m).wait_send()
+        nrm_pair(m).wait_send()
     for k in range(1, ntp):
         fin_copy(k).wait_send()
     for up in (True, False):
@@ -369,7 +431,6 @@
 def on_device(residual, lifted, dts, fades, long_rate, short_rate, long_freq, short_freq,
               long_lin, short_lin, skip, closing, emitted, leading, raising, lowering):
     nsp, ntp = lax.axis_size("sp"), lax.axis_size("tp")
-    rank = lax.axis_index("tp")
     n, W = lifted.shape
     G = dts.shape[0]
     half = G // 2
@@ -377,19 +438,7 @@
     S = half * (PL + PS)
     D = emitted.shape[1]
     Dl = residual.shape[1]
-    L, q = n // SUB, n // ntp
-
-    def owned(array, axis, count):
-        return lax.dynamic_slice_in_dim(array, rank * count, count, axis)
-
-    x = lifted.reshape(SUB, L, W).transpose(1, 0, 2).reshape(n, W)
-    mix = lambda a: a.reshape(G, SUB, L).transpose(2, 1, 0).reshape(n, G)
-    flat = lambda a, b: jnp.concatenate(
-        [owned(a, 1, half).reshape(2, -1), owned(b, 1, half).reshape(2, -1)], axis=1)
-    rates = jnp.stack([flat(long_rate, short_rate), flat(long_freq, short_freq)], axis=1).reshape(4, S)
-    lin = jnp.concatenate(
-        [owned(long_lin, 3, half).reshape(8, half * PL, CHAN),
-         owned(short_lin, 3, half).reshape(8, half * PS, CHAN)], axis=1)
+    q = n // ntp
     c_ff = min(nsp, raising.shape[1] // 128)
     F = raising.shape[1] // c_ff
     q_all, M = c_ff * q, ntp // 2
@@ -399,9 +448,10 @@
     return pl.pallas_call(
         functools.partial(mixer_body, cfg),
         out_shape=jax.ShapeDtypeStruct((n, Dl), BF16),
-        in_specs=[vm] * 9 + [pl.BlockSpec(memory_space=pl.ANY)] * 3,
+        in_specs=[vm] * 11 + [pl.BlockSpec(memory_space=pl.ANY)] * 5,
         out_specs=vm,
         scratch_shapes=[
+            pltpu.VMEM((8, half, CHAN, PL), F32), pltpu.VMEM((8, half, CHAN, PS), F32), dma((2, 8)),
             pltpu.VMEM((n, S), F32), pltpu.VMEM((n, S), F32),
             pltpu.VMEM((n, 4 * S), F32), pltpu.VMEM((n, 4 * S), F32),
             pltpu.VMEM((8, SUB, S), F32), pltpu.VMEM((8, S), F32), pltpu.VMEM((nsp - 1, 8, S), F32),
@@ -417,12 +467,12 @@
             dma((3,)), dma((nsp - 1,)), dma((nsp - 1,)), dma((ntp - 1,)), dma((ntp - 1,)),
             dma((ntp - 1,)), dma((ntp - 1,)),
             *[dma((nsp - 1,))] * 4, *[dma((M - 1, nsp))] * 4, *[dma((M,))] * 4,
-            *[dma((c_ff - 1,))] * 4, *[dma((ntp - 1,))] * 2,
+            *[dma((2, c_ff // 2))] * 2, *[dma((c_ff - 1,))] * 2, *[dma((ntp - 1,))] * 2,
         ],
         compiler_params=pltpu.CompilerParams(collective_id=0, has_side_effects=True),
         cost_estimate=pl.CostEstimate(flops=10**9, bytes_accessed=3 * 10**7, transcendentals=10**6),
-    )(x, mix(dts), mix(fades), rates, lin, owned(skip, 0, W)[None], owned(closing, 0, W)[None],
-      residual, leading[None], emitted, raising, lowering)
+    )(lifted, dts, fades, long_rate, short_rate, long_freq, short_freq, skip[None], closing[None],
+      residual, leading[None], long_lin.swapaxes(4, 5), short_lin.swapaxes(4, 5), emitted, raising, lowering)
 
 
 def solution(mesh):

time: 128 us -> 116 us (0.906)
  local copies, waits for them, and re-layouts: 12.9 us -> 1.57 us
    dynamic_slice x8 -> x0, local copies, waits for them, and re-layouts: 5.59 us -> none  [owned(): return lax.dynamic_slice_in_dim(array, rank * count, count, axis)]
    reshape x12 -> x0, local copies, waits for them, and re-layouts: 3.49 us -> none  [the longest x4 1.59 us: on_device(): mix = lambda a: a.reshape(G, SUB, L).transpose(2, 1, 0).reshape(n, G)]
    concatenate x1 -> x0, local copies, waits for them, and re-layouts: 2.18 us -> none  [on_device(): jnp.concatenate([owned(long_lin, 3, half).reshape(8, half * PL, CHAN), ow...]
where the time goes in v2:
time: 116 us
  Pallas kernels  114 us (98%)
  local copies, waits for them, and re-layouts  1.57 us (1%)
    pallas_call x1, Pallas kernels, on_device(): pl.pallas_call(functools.partial(mixer_body, cfg), out_shape=jax.ShapeDty...  114 us

profile of v2, /device:TPU:31, one launch (start us, length us, event | category | flops | bytes accessed | tf_op | source)
XLA Modules:
  0.0 115.9 jit_solution(8036080370142358697)
XLA Ops:
  0.0 114.3 %shard_map.154 = bf16[128,512]{1,0:T(8,128)(2,1)} custom-call(bf16[128,256]{1,0:T(8,128)(2,1)} %x_ref.1, f32[16,128]{1,0:T(8,128)} %dt_ref.1, f32[16,128]{1,0:T(8,128)} %lf_ref.1, f32[2,32,64]{2,1,0:T(8,128)} %long_rate.1, f32[2,32,32]{2,1,0:T(8,128)} %short_rate.1, f32[2,32,64]{2,1,0:T(8,128)} %long_freq.1, f32[2,32,32]{2,1,0:T(8,128)} %short_freq.1, ...), custom_call_target="tpu_custom_call" | custom-call | flops 1000000000 | bytes 30000000 | tf_op jit(solution)/shard_map/pallas_call | solution.py:448
  114.3 1.6 %copy.18 = bf16[128,512]{1,0:T(8,128)(2,1)} copy(bf16[128,512]{1,0:T(8,128)(2,1)} %shard_map.154) | data formatting | bytes 262144
